TPU v7x, 32 devices: a whole 2x2x4 slice. The times are simulated.
32 devices in a mesh: sp: 4 (over y, x), tp: 8 (over z, core).
Axes of the slice: x: 2, y: 2, z: 4, core: 2. Of those that a mesh axis runs over, the one named last changes fastest.
Arguments:
- upstream: bfloat16 [1024, 4096], P('sp', 'tp'), may hold values from -6 to 6
- stream: bfloat16 [1024, 4096], P('sp', 'tp'), may hold values from -400 to 400
- norm_gain: float32 [4096], P('tp'), may hold values from 0.1 to 1.9
- routes: int32 [1024, 2], P('sp'), may hold values from 0 to 3, all different within a row; in each aligned block of 256 rows (0 to 255, 256 to 511, ...) at most 192 rows name the same one
- route_weights: float32 [1024, 2], P('sp'), may hold values from 0.1 to 1
- w_gate: bfloat16 [4, 4096, 2048], P('sp', None, 'tp'), may hold values from -0.09375 to 0.09375
- w_up: bfloat16 [4, 4096, 2048], P('sp', None, 'tp'), may hold values from -0.09375 to 0.09375
- w_down: bfloat16 [4, 2048, 4096], P('sp', 'tp'), may hold values from -0.125 to 0.125
- value_in: bfloat16 [1024, 2048], P('sp', 'tp'), may hold values from -6 to 6
- gate_in: bfloat16 [1024, 2048], P('sp', 'tp'), may hold values from -6 to 6
- conv_pre: bfloat16 [1024, 2048], P('sp', 'tp'), may hold values from -200 to 200
- ln_gain: float32 [2048], P('tp'), may hold values from 0.1 to 1.9
- conv_taps: float32 [31, 2048], P(None, 'tp'), may hold values from -1 to 1
- w_out: bfloat16 [2048, 4096], P('tp'), may hold values from -0.125 to 0.125
Outputs:
- grad_gate: float32 [4, 4096, 2048], P('sp', None, 'tp')
- grad_up: float32 [4, 4096, 2048], P('sp', None, 'tp')
- grad_down: float32 [4, 2048, 4096], P('sp', 'tp')
- grad_out: float32 [2048, 4096], P('tp', 'sp')
- value_grad: bfloat16 [1024, 2048], P('sp', 'tp')
- gate_grad: bfloat16 [1024, 2048], P('sp', 'tp')
Inputs may be any that keep to these rules, and one draw needn't show every extreme that they name: `routes`: each token names two different experts. Among the tokens of one index of sp no expert is named more than 192 times, and in every draw some expert exactly 192 times.
All inputs are finite; a program needn't handle non-finite values.
Results may differ from a plain program's by a relative error of at most 0.0071.
Values may be sent and summed in bfloat16 or wider, within the bound.
A program may use at most 128 MiB of HBM per device.

v0:
```python
import jax
import jax.numpy as jnp
from jax import lax
from jax.sharding import PartitionSpec as P

EPSILON = 1e-06


def shifted(block, axis, distance):
    devices = range(lax.axis_size(axis))
    route = [(i - distance, i) for i in devices if i - distance in devices]
    return lax.ppermute(block, axis, route)


def silu_slope(values):
    logistic = jax.nn.sigmoid(values)
    return logistic * (1.0 + values * (1.0 - logistic))


def per_device(
    upstream,
    stream,
    norm_gain,
    routes,
    route_weights,
    w_gate,
    w_up,
    w_down,
    value_in,
    gate_in,
    conv_pre,
    ln_gain,
    conv_taps,
    w_out,
):
    tok_rows, width_part = stream.shape
    token_groups = lax.axis_size("sp")
    width_groups = lax.axis_size("tp")
    model_width = width_part * width_groups
    channels = conv_pre.shape[1] * width_groups
    tap_count = conv_taps.shape[0]
    capacity = 3 * tok_rows // token_groups
    experts = w_gate.shape[0] * token_groups
    slot_count = experts * capacity
    expert_rows = token_groups * capacity
    residual = stream.astype(jnp.float32)
    conv_vals = conv_pre.astype(jnp.float32)
    row_squares, conv_total, conv_squares = lax.psum(
        (
            jnp.sum(residual * residual, axis=1),
            jnp.sum(conv_vals, axis=1),
            jnp.sum(conv_vals * conv_vals, axis=1),
        ),
        "tp",
    )
    inverse = lax.rsqrt(row_squares / model_width + EPSILON)[:, None]
    normed = (norm_gain[None, :] * residual * inverse).astype(jnp.bfloat16)
    flat_experts = routes.reshape(-1)
    one_hot = (flat_experts[:, None] == jnp.arange(experts, dtype=jnp.int32)[None, :]).astype(
        jnp.int32
    )
    slot_rank = jnp.sum((jnp.cumsum(one_hot, axis=0) - one_hot) * one_hot, axis=1)
    slot_index = (flat_experts * capacity + slot_rank).reshape(tok_rows, 2)
    slot_ids = jnp.arange(slot_count, dtype=jnp.int32)[:, None]
    first_hit = slot_ids == slot_index[None, :, 0]
    second_hit = slot_ids == slot_index[None, :, 1]
    any_hit = jnp.logical_or(first_hit, second_hit)
    picker = any_hit.astype(jnp.bfloat16)
    slot_weight = jnp.sum(
        jnp.where(first_hit, route_weights[None, :, 0], 0.0)
        + jnp.where(second_hit, route_weights[None, :, 1], 0.0),
        axis=1,
    )
    token_iota = jnp.arange(tok_rows, dtype=jnp.int32)[None, :]
    slot_token = jnp.where(
        jnp.any(any_hit, axis=1), jnp.sum(jnp.where(any_hit, token_iota, 0), axis=1), tok_rows
    )
    columns = normed.shape[1]
    normed_pad = jnp.concatenate([normed, jnp.zeros((1, columns), jnp.bfloat16)], axis=0)
    upstream_pad = jnp.concatenate([upstream, jnp.zeros((1, columns), jnp.bfloat16)], axis=0)
    inputs = normed_pad[slot_token]
    cotangent = (upstream_pad[slot_token].astype(jnp.float32) * slot_weight[:, None]).astype(
        jnp.bfloat16
    )
    sent_inputs = inputs.reshape(experts, capacity, columns)
    sent_cotangent = cotangent.reshape(experts, capacity, columns)
    part_inputs, part_cotangent = (
        lax.all_to_all(sent_inputs, "sp", split_axis=0, concat_axis=0, tiled=True),
        lax.all_to_all(sent_cotangent, "sp", split_axis=0, concat_axis=0, tiled=True),
    )
    inputs, cotangent = (
        lax.all_gather(part_inputs.reshape(expert_rows, width_part), "tp", axis=1, tiled=True),
        lax.all_gather(part_cotangent.reshape(expert_rows, width_part), "tp", axis=1, tiled=True),
    )
    gate_mat = w_gate[0]
    upper_mat = w_up[0]
    down_mat = w_down[0]
    gate_pre = jnp.dot(inputs, gate_mat, preferred_element_type=jnp.float32)
    upper_pre = jnp.dot(inputs, upper_mat, preferred_element_type=jnp.float32)
    active = (jax.nn.silu(gate_pre) * upper_pre).astype(jnp.bfloat16)
    active_back = lax.dot_general(
        cotangent, down_mat, (((1,), (1,)), ((), ())), preferred_element_type=jnp.float32
    )
    gate_back = (active_back * upper_pre * silu_slope(gate_pre)).astype(jnp.bfloat16)
    upper_back = (active_back * jax.nn.silu(gate_pre)).astype(jnp.bfloat16)
    grad_gate = lax.dot_general(
        inputs, gate_back, (((0,), (0,)), ((), ())), preferred_element_type=jnp.float32
    )
    grad_up = lax.dot_general(
        inputs, upper_back, (((0,), (0,)), ((), ())), preferred_element_type=jnp.float32
    )
    grad_down = lax.dot_general(
        active, cotangent, (((0,), (0,)), ((), ())), preferred_element_type=jnp.float32
    )
    input_part = lax.dot_general(
        gate_back, gate_mat, (((1,), (1,)), ((), ())), preferred_element_type=jnp.float32
    ) + lax.dot_general(
        upper_back, upper_mat, (((1,), (1,)), ((), ())), preferred_element_type=jnp.float32
    )
    input_back = lax.psum_scatter(input_part, "tp", scatter_dimension=1, tiled=True).astype(
        jnp.bfloat16
    )
    returned = lax.all_to_all(
        input_back.reshape(token_groups, capacity, width_part),
        "sp",
        split_axis=0,
        concat_axis=0,
        tiled=True,
    )
    returned = returned.reshape(slot_count, width_part)
    token_back = lax.dot_general(
        picker, returned, (((0,), (0,)), ((), ())), preferred_element_type=jnp.float32
    )
    gained = norm_gain[None, :] * token_back
    inner_sum = lax.psum(jnp.sum(gained * residual, axis=1), "tp")
    norm_back = inverse * gained - residual * inverse**3 * (inner_sum / model_width)[:, None]
    stream_grad = (upstream.astype(jnp.float32) + norm_back).astype(jnp.bfloat16)
    full_grad = lax.all_gather(stream_grad, "tp", axis=1, tiled=True)
    mean_val = (conv_total / channels)[:, None]
    variance = (conv_squares / channels)[:, None] - mean_val * mean_val
    inv_std = lax.rsqrt(variance + EPSILON)
    centred = (conv_vals - mean_val) * inv_std
    scaled = centred * ln_gain[None, :]
    mixed_out = jax.nn.silu(scaled).astype(jnp.bfloat16)
    columns = full_grad
    grad_rows = lax.psum_scatter(
        lax.dot_general(
            columns, mixed_out, (((0,), (0,)), ((), ())), preferred_element_type=jnp.float32
        ),
        "sp",
        scatter_dimension=0,
        tiled=True,
    )
    grad_out = grad_rows.T
    mixed_back = lax.dot_general(
        full_grad, w_out, (((1,), (1,)), ((), ())), preferred_element_type=jnp.float32
    )
    norm_in = mixed_back * silu_slope(scaled) * ln_gain[None, :]
    norm_total, norm_cross = lax.psum(
        (jnp.sum(norm_in, axis=1), jnp.sum(norm_in * centred, axis=1)), "tp"
    )
    conv_back = inv_std * (
        norm_in - (norm_total / channels)[:, None] - centred * (norm_cross / channels)[:, None]
    )
    next_rim = shifted(conv_back[: tap_count - 1], "sp", -1)
    padded = jnp.concatenate([conv_back, next_rim], axis=0)
    glu_back = jnp.zeros(conv_back.shape, jnp.float32)
    for tap_index in range(tap_count):
        offset = tap_count - 1 - tap_index
        glu_back = glu_back + conv_taps[tap_index][None, :] * padded[offset : offset + tok_rows]
    gate_sigma = jax.nn.sigmoid(gate_in.astype(jnp.float32))
    value_grad = (glu_back * gate_sigma).astype(jnp.bfloat16)
    gate_grad = (glu_back * value_in.astype(jnp.float32) * gate_sigma * (1.0 - gate_sigma)).astype(
        jnp.bfloat16
    )
    return (grad_gate[None], grad_up[None], grad_down[None], grad_out, value_grad, gate_grad)


def solution(mesh):
    return jax.shard_map(
        per_device,
        mesh=mesh,
        in_specs=(
            P("sp", "tp"),
            P("sp", "tp"),
            P("tp"),
            P("sp", None),
            P("sp", None),
            P("sp", None, "tp"),
            P("sp", None, "tp"),
            P("sp", "tp", None),
            P("sp", "tp"),
            P("sp", "tp"),
            P("sp", "tp"),
            P("tp"),
            P(None, "tp"),
            P("tp", None),
        ),
        out_specs=(
            P("sp", None, "tp"),
            P("sp", None, "tp"),
            P("sp", "tp", None),
            P("tp", "sp"),
            P("sp", "tp"),
            P("sp", "tp"),
        ),
        check_vma=False,
    )
```

profile of v0, /device:TPU:0, one launch (start us, length us, event | category | flops | bytes accessed | tf_op | source)
XLA Modules:
  0.0 439.3 jit_solution(1147835568961126519)
XLA Ops:
  12.7 18.1 %psum.42 = f32[256]{0:T(256)S(1)} all-reduce(f32[256]{0:T(256)S(1)} %fusion.15), channel_id=1, replica_groups=mesh['sp'=4,'tp'=8] {'tp'}, use_global_device_ids=true, to_apply=%region_1.0 | all-reduce | flops 256 | bytes 2048 | tf_op jit(solution)/shard_map/psum | solution.py:48
  31.9 2.7 gather_fusion
  34.6 12.2 %all_to_all.15 = bf16[4,192,512]{2,1,0:T(8,128)(2,1)} all-to-all(bf16[4,192,512]{2,1,0:T(8,128)(2,1)S(1)} %bitcast.98), channel_id=1, replica_groups=mesh['sp'=4,'tp'=8] {'sp'}, dimensions={0} | all-to-all | bytes 1572864 | tf_op jit(solution)/shard_map/all_to_all | solution.py:88
  46.9 2.7 gather_fusion.1
  50.1 11.6 %all_to_all.16 = bf16[4,192,512]{2,1,0:T(8,128)(2,1)} all-to-all(bf16[4,192,512]{2,1,0:T(8,128)(2,1)S(1)} %fusion.9), channel_id=1, replica_groups=mesh['sp'=4,'tp'=8] {'sp'}, dimensions={0} | all-to-all | bytes 1572864 | tf_op jit(solution)/shard_map/all_to_all | solution.py:89
  62.1 47.4 %all-gather.4.cloned.1.call-done = bf16[768,4096]{1,0:T(8,128)(2,1)} async-done(((bf16[768,512]{1,0:T(8,128)(2,1)}), bf16[768,4096]{1,0:T(8,128)(2,1)}) %all-gather.4.cloned.1.call-update) | async-done | bytes 6291472 | tf_op jit(solution)/shard_map/all_gather | solution.py:92
  109.4 4.7 %fusion.2 = f32[768,256]{1,0:T(8,128)S(1)} fusion(bf16[768,4096]{1,0:T(8,128)(2,1)} %all-gather.4.cloned.1.call-done, bf16[1,4096,256]{2,1,0:T(8,128)(2,1)S(1)} %copy-done), kind=kOutput, calls=%fused_computation.37 | convolution fusion | flops 1610612736 | bytes 9175040 | tf_op jit(solution)/shard_map/dot_general | solution.py:98
  114.6 2.7 fusion.5
  117.3 57.1 %all-gather.6.cloned.1.call-done = bf16[768,4096]{1,0:T(8,128)(2,1)} async-done(((bf16[768,512]{1,0:T(8,128)(2,1)}), bf16[768,4096]{1,0:T(8,128)(2,1)}) %all-gather.6.cloned.1.call-update) | async-done | bytes 6291472 | tf_op jit(solution)/shard_map/all_gather | solution.py:93
  174.4 5.5 %multiply_convert_fusion.1 = (bf16[768,256]{1,0:T(8,128)(2,1)S(1)}, bf16[768,256]{1,0:T(8,128)(2,1)S(1)}) fusion(f32[768,256]{1,0:T(8,128)S(1)} %fusion.2, f32[768,256]{1,0:T(8,128)} %fusion.5, bf16[768,4096]{1,0:T(8,128)(2,1)} %all-gather.6.cloned.1.call-done, bf16[1,256,4096]{2,1,0:T(8,128)(2,1)} %param.21), kind=kOutput, calls=%fused_computation.54 | convolution fusion | flops 1613168640 | bytes 10747904 | tf_op jit(solution)/shard_map/dot_general | solution.py:101
  181.8 6.4 %convolution_add_fusion = f32[768,4096]{1,0:T(8,128)} fusion(f32[768,4096]{1,0:T(8,128)S(1)} %fusion, bf16[768,256]{1,0:T(8,128)(2,1)S(1)} %get-tuple-element.47, bf16[1,4096,256]{2,1,0:T(8,128)(2,1)S(1)} %copy-done.5), kind=kOutput, calls=%fused_computation.2 | convolution fusion | flops 1613758464 | bytes 27656192 | tf_op jit(solution)/shard_map/dot_general | solution.py:117
  188.3 127.9 %reduce-scatter.3.cloned.1.call-done = f32[768,512]{1,0:T(8,128)} async-done(((f32[768,4096]{1,0:T(8,128)}), f32[768,512]{1,0:T(8,128)}) %reduce-scatter.3.cloned.1.call-update) | async-done | bytes 1572880 | tf_op jit(solution)/shard_map/reduce_scatter | solution.py:120
  316.2 2.4 convert_element_type.72
  318.6 3.6 all-to-all-start.2
  322.4 8.9 %all-to-all-done.2 = bf16[4,192,512]{2,1,0:T(8,128)(2,1)S(1)} async-done(((bf16[4,192,512]{2,1,0:T(8,128)(2,1)}), bf16[4,192,512]{2,1,0:T(8,128)(2,1)S(1)}, u32[]{:S(2)}, u32[]{:S(2)}) %all-to-all-start.2) | async-done | bytes 786464 | tf_op jit(solution)/shard_map/all_to_all | solution.py:123
  331.8 14.8 %all-reduce.3 = (f32[256]{0:T(256)S(1)}, f32[256]{0:T(256)S(1)}, f32[256]{0:T(256)S(1)}) all-reduce(f32[256]{0:T(256)S(1)} %get-tuple-element.88, f32[256]{0:T(256)S(1)} %get-tuple-element.39, f32[256]{0:T(256)S(1)} %get-tuple-element.38), channel_id=1, replica_groups=mesh['sp'=4,'tp'=8] {'tp'}, use_global_device_ids=true, to_apply=%region_10.11 | all-reduce | flops 768 | bytes 6144 | tf_op jit(solution)/shard_map/psum | solution.py:135
  347.9 25.8 %all-gather.8.cloned.1.call-done = bf16[256,4096]{1,0:T(8,128)(2,1)} async-done(((bf16[256,512]{1,0:T(8,128)(2,1)}), bf16[256,4096]{1,0:T(8,128)(2,1)}) %all-gather.8.cloned.1.call-update) | async-done | bytes 2097168 | tf_op jit(solution)/shard_map/all_gather | solution.py:138
  373.7 4.4 fusion.132
  379.1 6.7 %convolution_bitcast_fusion.2 = f32[1,4096,256]{2,1,0:T(8,128)} fusion(bf16[768,4096]{1,0:T(8,128)(2,1)} %all-gather.4.cloned.1.call-done, bf16[768,256]{1,0:T(8,128)(2,1)S(1)} %copy-done.12), kind=kOutput, calls=%fused_computation.5 | convolution fusion | flops 1610612736 | bytes 10878976 | tf_op jit(solution)/shard_map/dot_general | solution.py:106
  385.8 6.9 %convolution_bitcast_fusion = f32[1,256,4096]{2,1,0:T(8,128)} fusion(bf16[768,4096]{1,0:T(8,128)(2,1)} %all-gather.6.cloned.1.call-done, f32[768,256]{1,0:T(8,128)S(1)} %copy-done.6, f32[768,256]{1,0:T(8,128)S(1)} %fusion.2), kind=kOutput, calls=%fused_computation.3 | convolution fusion | flops 1611792384 | bytes 12058624 | tf_op jit(solution)/shard_map/dot_general | solution.py:112
  393.6 15.3 %all-reduce.2 = (f32[256]{0:T(256)S(1)}, f32[256]{0:T(256)S(1)}) all-reduce(f32[256]{0:T(256)S(1)} %get-tuple-element.37, f32[256]{0:T(256)S(1)} %get-tuple-element.36), channel_id=1, replica_groups=mesh['sp'=4,'tp'=8] {'tp'}, use_global_device_ids=true, to_apply=%region_19.20 | all-reduce | flops 512 | bytes 4096 | tf_op jit(solution)/shard_map/psum | solution.py:159
  410.6 6.8 %convolution_bitcast_fusion.1 = f32[1,4096,256]{2,1,0:T(8,128)} fusion(bf16[768,4096]{1,0:T(8,128)(2,1)} %all-gather.4.cloned.1.call-done, bf16[768,256]{1,0:T(8,128)(2,1)S(1)} %get-tuple-element.47), kind=kOutput, calls=%fused_computation.4 | convolution fusion | flops 1610612736 | bytes 10878976 | tf_op jit(solution)/shard_map/dot_general | solution.py:109
  420.2 10.0 %reduce-scatter.5.cloned.1.call-done = f32[1024,256]{1,0:T(8,128)} async-done(((f32[4096,256]{1,0:T(8,128)}), f32[1024,256]{1,0:T(8,128)}) %reduce-scatter.5.cloned.1.call-update) | async-done | bytes 1048592 | tf_op jit(solution)/shard_map/reduce_scatter | solution.py:146
  430.2 2.5 copy.39
  (93 shorter events, 18.0 us)
Async XLA Ops:
  7.2 102.2 %copy-start = (bf16[1,4096,256]{2,1,0:T(8,128)(2,1)S(1)}, bf16[1,4096,256]{2,1,0:T(8,128)(2,1)}, u32[]{:S(2)}) copy-start(bf16[1,4096,256]{2,1,0:T(8,128)(2,1)} %param.19) | copy-start | bytes 6291460
  7.2 102.2 %all-gather.4.cloned.1.call-start = ((), (), s32[]{:S(2)}) async-start(), calls=%async_computation.5 | async-start | bytes 7077888 | tf_op jit(solution)/shard_map/all_gather | solution.py:92
  31.9 14.9 %copy-start.8 = (bf16[256,512]{1,0:T(8,128)(2,1)S(1)}, bf16[256,512]{1,0:T(8,128)(2,1)}, u32[]{:S(2)}) copy-start(bf16[256,512]{1,0:T(8,128)(2,1)} %param.14) | copy-start | bytes 786436
  46.8 2.8 copy-start.16
  46.8 127.6 %all-gather.6.cloned.1.call-start = ((), (), s32[]{:S(2)}) async-start(), calls=%async_computation.6 | async-start | bytes 7077888 | tf_op jit(solution)/shard_map/all_gather | solution.py:93
  61.8 254.4 %reduce-scatter.3.cloned.1.call-start = ((), (), s32[]{:S(2)}) async-start(), calls=%async_computation.7 | async-start | bytes 14155776 | tf_op jit(solution)/shard_map/reduce_scatter | solution.py:120
  109.4 4.7 %copy-start.4 = (bf16[1,4096,256]{2,1,0:T(8,128)(2,1)S(1)}, bf16[1,4096,256]{2,1,0:T(8,128)(2,1)}, u32[]{:S(2)}) copy-start(bf16[1,4096,256]{2,1,0:T(8,128)(2,1)} %param.20) | copy-start | bytes 6291460
  109.4 5.2 %copy-start.18 = (bf16[768,4096]{1,0:T(8,128)(2,1)S(1)}, bf16[768,4096]{1,0:T(8,128)(2,1)}, u32[]{:S(2)}) copy-start(bf16[768,4096]{1,0:T(8,128)(2,1)} %all-gather.4.cloned.1.call-done) | copy-start | bytes 18874372
  179.9 1.9 copy-start.11
  188.2 134.0 %copy-start.7 = (bf16[256,256]{1,0:T(8,128)(2,1)S(1)}, bf16[256,256]{1,0:T(8,128)(2,1)}, u32[]{:S(2)}) copy-start(bf16[256,256]{1,0:T(8,128)(2,1)} %param.24) | copy-start | bytes 393220
  188.2 143.1 %copy-start.3 = (bf16[256,512]{1,0:T(8,128)(2,1)S(1)}, bf16[256,512]{1,0:T(8,128)(2,1)}, u32[]{:S(2)}) copy-start(bf16[256,512]{1,0:T(8,128)(2,1)} %param.15) | copy-start | bytes 786436
  188.2 143.1 %copy-start.15 = (f32[512]{0:T(512)S(1)}, f32[512]{0:T(512)}, u32[]{:S(2)}) copy-start(f32[512]{0:T(512)} %param.16) | copy-start | bytes 6148
  188.2 158.4 %copy-start.9 = (bf16[256,512]{1,0:T(8,128)(2,1)S(1)}, bf16[256,512]{1,0:T(8,128)(2,1)}, u32[]{:S(2)}) copy-start(bf16[256,512]{1,0:T(8,128)(2,1)} %param.14) | copy-start | bytes 786436
  188.2 185.5 %copy-start.17 = (f32[256]{0:T(256)S(1)}, f32[256]{0:T(256)}, u32[]{:S(2)}) copy-start(f32[256]{0:T(256)} %param.25) | copy-start | bytes 3076
  318.6 12.7 %all-to-all-start.2 = ((bf16[4,192,512]{2,1,0:T(8,128)(2,1)}), bf16[4,192,512]{2,1,0:T(8,128)(2,1)S(1)}, u32[]{:S(2)}, u32[]{:S(2)}) async-start(bf16[4,192,512]{2,1,0:T(8,128)(2,1)} %bitcast.15), calls=%async_computation.3 | async-start | bytes 1572864 | tf_op jit(solution)/shard_map/all_to_all | solution.py:123
  322.2 51.5 %all-gather.8.cloned.1.call-start = ((), (), s32[]{:S(2)}) async-start(), calls=%async_computation.8 | async-start | bytes 2359296 | tf_op jit(solution)/shard_map/all_gather | solution.py:138
  347.6 82.7 %reduce-scatter.5.cloned.1.call-start = ((), (), s32[]{:S(2)}) async-start(), calls=%async_computation.9 | async-start | bytes 5242880 | tf_op jit(solution)/shard_map/reduce_scatter | solution.py:146
  379.1 6.7 %copy-start.6 = (f32[768,256]{1,0:T(8,128)S(1)}, f32[768,256]{1,0:T(8,128)}, u32[]{:S(2)}) copy-start(f32[768,256]{1,0:T(8,128)} %fusion.5) | copy-start | bytes 2359300
  385.8 6.9 %copy-start.2 = (bf16[256,4096]{1,0:T(8,128)(2,1)S(1)}, bf16[256,4096]{1,0:T(8,128)(2,1)}, u32[]{:S(2)}) copy-start(bf16[256,4096]{1,0:T(8,128)(2,1)} %all-gather.8.cloned.1.call-done) | copy-start | bytes 6291460
  385.8 6.9 %copy-start.19 = (bf16[256,4096]{1,0:T(8,128)(2,1)S(1)}, bf16[256,4096]{1,0:T(8,128)(2,1)}, u32[]{:S(2)}) copy-start(bf16[256,4096]{1,0:T(8,128)(2,1)} %param.27) | copy-start | bytes 6291460
  409.2 8.3 %copy-start.10 = (bf16[256,256]{1,0:T(8,128)(2,1)S(1)}, bf16[256,256]{1,0:T(8,128)(2,1)}, u32[]{:S(2)}) copy-start(bf16[256,256]{1,0:T(8,128)(2,1)} %param.23) | copy-start | bytes 393220
  409.2 8.3 %copy-start.13 = (bf16[256,256]{1,0:T(8,128)(2,1)S(1)}, bf16[256,256]{1,0:T(8,128)(2,1)}, u32[]{:S(2)}) copy-start(bf16[256,256]{1,0:T(8,128)(2,1)} %param.22) | copy-start | bytes 393220
  409.2 8.2 %collective-permute-start = (f32[30,256]{1,0:T(8,128)S(1)}, f32[30,256]{1,0:T(8,128)S(1)}, u32[]{:S(2)}, u32[]{:S(2)}) collective-permute-start(f32[30,256]{1,0:T(8,128)S(1)} %slice.279), channel_id=1, source_target_pairs={{8,0},{16,8},{24,16},{9,1},{17,9},{25,17},{10,2},{18,10},{26,18},{... | collective-permute-start | bytes 92168 | tf_op jit(solution)/shard_map/ppermute | solution.py:12
  410.6 22.2 %copy-start.1 = (bf16[1,4096,256]{2,1,0:T(8,128)(2,1)S(1)}, bf16[1,4096,256]{2,1,0:T(8,128)(2,1)}, u32[]{:S(2)}) copy-start(bf16[1,4096,256]{2,1,0:T(8,128)(2,1)} %param.19) | copy-start | bytes 6291460
  (3 other events, 3.6 us)
Sparse Core Ops, SparseCore 0:
  46.9 62.4 all-gather.3
  111.0 63.3 all-gather.5
  188.4 127.7 reduce-scatter.2
  347.7 25.9 all-gather.7
  378.2 51.9 reduce-scatter.4
where the time goes:
time: 440 us; the launch traced here: 439 us
  waiting for transfers between devices  277 us (63%)
  blocking collectives  72 us (16%)
  matrix products  47.3 us (11%)
  between operations  14.1 us (3%)
  other arithmetic  11.8 us (3%)
  local copies, waits for them, and re-layouts  11.2 us (3%)
  starting transfers between devices  5.63 us (1%)
    reduce_scatter x1, waiting for transfers between devices, per_device(): lax.psum_scatter(input_part, 'tp', scatter_dimension=1, tiled=True)  128 us
    all_gather x1, waiting for transfers between devices, per_device(): lax.all_gather(part_cotangent.reshape(expert_rows, width_part), 'tp', axi...  57.1 us
    all_gather x1, waiting for transfers between devices, per_device(): lax.all_gather(part_inputs.reshape(expert_rows, width_part), 'tp', axis=1...  47.4 us
    all_gather x1, waiting for transfers between devices, per_device(): full_grad = lax.all_gather(stream_grad, 'tp', axis=1, tiled=True)  25.8 us
    psum x1, blocking collectives, per_device(): lax.psum((jnp.sum(residual * residual, axis=1), jnp.sum(conv_vals, axis=1...  18.1 us
    psum x1, blocking collectives, per_device(): lax.psum((jnp.sum(norm_in, axis=1), jnp.sum(norm_in * centred, axis=1)),...  15.3 us
    psum x1, blocking collectives, per_device(): inner_sum = lax.psum(jnp.sum(gained * residual, axis=1), 'tp')  14.8 us
    all_to_all x1, blocking collectives, per_device(): lax.all_to_all(sent_inputs, 'sp', split_axis=0, concat_axis=0, tiled=True)  12.2 us
  transfers between devices with their start and end apart: 7, of which 6 were waited for; matrix products, arithmetic and copies ran while one was open for 8% of the time, Pallas kernels for 0%

commit v1 on v0

--- a/solution.py
+++ b/solution.py
@@ -90,7 +90,15 @@
     )
     inputs, cotangent = (
         lax.all_gather(part_inputs.reshape(expert_rows, width_part), "tp", axis=1, tiled=True),
-        lax.all_gather(part_cotangent.reshape(expert_rows, width_part), "tp", axis=1, tiled=True),
+        jnp.concatenate(
+            lax.all_to_all(
+                jnp.stack([part_cotangent.reshape(expert_rows, width_part)] * lax.axis_size("tp")),
+                "tp",
+                0,
+                0,
+            ),
+            axis=1,
+        ),
     )
     gate_mat = w_gate[0]
     upper_mat = w_up[0]

time: 440 us -> 508 us (1.15)
  waiting for transfers between devices: 277 us -> 334 us
  starting transfers between devices: 5.63 us -> 12 us
    all_to_all x0 -> x1, waiting for transfers between devices: none -> 93.6 us  [per_device(): lax.all_to_all(jnp.stack([part_cotangent.reshape(expert_rows, width_part)...]
    all_gather x1 -> x0, waiting for transfers between devices: 57.1 us -> none  [per_device(): lax.all_gather(part_cotangent.reshape(expert_rows, width_part), 'tp', axi...]
    all_gather x1, waiting for transfers between devices: 47.4 us -> 67.6 us  [per_device(): lax.all_gather(part_inputs.reshape(expert_rows, width_part), 'tp', axis=1...]
    all_to_all x0 -> x1, starting transfers between devices: none -> 6.44 us  [per_device(): lax.all_to_all(jnp.stack([part_cotangent.reshape(expert_rows, width_part)...]
where the time goes in v1:
time: 508 us
  waiting for transfers between devices  334 us (66%)
  blocking collectives  72 us (14%)
  matrix products  48.6 us (10%)
  local copies, waits for them, and re-layouts  15.2 us (3%)
  between operations  14.1 us (3%)
  starting transfers between devices  12 us (2%)
  other arithmetic  11.8 us (2%)
    reduce_scatter x1, waiting for transfers between devices, per_device(): lax.psum_scatter(input_part, 'tp', scatter_dimension=1, tiled=True)  128 us
    all_to_all x1, waiting for transfers between devices, per_device(): lax.all_to_all(jnp.stack([part_cotangent.reshape(expert_rows, width_part)...  93.6 us
    all_gather x1, waiting for transfers between devices, per_device(): lax.all_gather(part_inputs.reshape(expert_rows, width_part), 'tp', axis=1...  67.6 us
    all_gather x1, waiting for transfers between devices, per_device(): full_grad = lax.all_gather(stream_grad, 'tp', axis=1, tiled=True)  25.9 us
    psum x1, blocking collectives, per_device(): lax.psum((jnp.sum(residual * residual, axis=1), jnp.sum(conv_vals, axis=1...  18.1 us
    psum x1, blocking collectives, per_device(): lax.psum((jnp.sum(norm_in, axis=1), jnp.sum(norm_in * centred, axis=1)),...  15.3 us
    psum x1, blocking collectives, per_device(): inner_sum = lax.psum(jnp.sum(gained * residual, axis=1), 'tp')  14.8 us
    all_to_all x1, blocking collectives, per_device(): lax.all_to_all(sent_inputs, 'sp', split_axis=0, concat_axis=0, tiled=True)  12.2 us
  transfers between devices with their start and end apart: 7, of which 6 were waited for; matrix products, arithmetic and copies ran while one was open for 8% of the time, Pallas kernels for 0%

profile of v1, /device:TPU:0, one launch (start us, length us, event | category | flops | bytes accessed | tf_op | source)
XLA Modules:
  0.0 507.7 jit_solution(7902687879120564604)
XLA Ops:
  12.7 18.1 %psum.42 = f32[256]{0:T(256)S(1)} all-reduce(f32[256]{0:T(256)S(1)} %fusion.15), channel_id=1, replica_groups=mesh['sp'=4,'tp'=8] {'tp'}, use_global_device_ids=true, to_apply=%region_1.0 | all-reduce | flops 256 | bytes 2048 | tf_op jit(solution)/shard_map/psum | solution.py:48
  31.9 2.7 gather_fusion
  34.6 12.2 %all_to_all.20 = bf16[4,192,512]{2,1,0:T(8,128)(2,1)} all-to-all(bf16[4,192,512]{2,1,0:T(8,128)(2,1)S(1)} %bitcast.101), channel_id=1, replica_groups=mesh['sp'=4,'tp'=8] {'sp'}, dimensions={0} | all-to-all | bytes 1572864 | tf_op jit(solution)/shard_map/all_to_all | solution.py:88
  46.8 2.7 gather_fusion.1
  50.1 11.7 %all_to_all.21 = bf16[4,192,512]{2,1,0:T(8,128)(2,1)} all-to-all(bf16[4,192,512]{2,1,0:T(8,128)(2,1)S(1)} %fusion.9), channel_id=1, replica_groups=mesh['sp'=4,'tp'=8] {'sp'}, dimensions={0} | all-to-all | bytes 1572864 | tf_op jit(solution)/shard_map/all_to_all | solution.py:89
  63.2 3.1 stack.3
  66.2 6.4 %all-to-all-start.2 = ((bf16[8,768,512]{1,2,0:T(8,128)(2,1)}), bf16[8,768,512]{1,2,0:T(8,128)(2,1)}, u32[]{:S(2)}, u32[]{:S(2)}) async-start(bf16[8,768,512]{1,2,0:T(8,128)(2,1)} %stack.3), calls=%async_computation.2 | async-start | bytes 12582912 | tf_op jit(solution)/shard_map/all_to_all | solution.py:94
  72.9 67.6 %all-gather.3.cloned.1.call-done = bf16[768,4096]{1,0:T(8,128)(2,1)} async-done(((bf16[768,512]{1,0:T(8,128)(2,1)}), bf16[768,4096]{1,0:T(8,128)(2,1)}) %all-gather.3.cloned.1.call-update) | async-done | bytes 6291472 | tf_op jit(solution)/shard_map/all_gather | solution.py:92
  140.5 5.6 %fusion.2 = f32[768,256]{1,0:T(8,128)} fusion(bf16[768,4096]{1,0:T(8,128)(2,1)} %all-gather.3.cloned.1.call-done, bf16[1,4096,256]{2,1,0:T(8,128)(2,1)S(1)} %copy-done), kind=kOutput, calls=%fused_computation.37 | convolution fusion | flops 1610612736 | bytes 9175040 | tf_op jit(solution)/shard_map/dot_general | solution.py:106
  146.1 2.7 fusion.5
  148.8 93.6 %all-to-all-done.2 = bf16[8,768,512]{1,2,0:T(8,128)(2,1)} async-done(((bf16[8,768,512]{1,2,0:T(8,128)(2,1)}), bf16[8,768,512]{1,2,0:T(8,128)(2,1)}, u32[]{:S(2)}, u32[]{:S(2)}) %all-to-all-start.2) | async-done | bytes 6291488 | tf_op jit(solution)/shard_map/all_to_all | solution.py:94
  242.4 5.7 %multiply_convert_fusion.1 = (bf16[768,256]{1,0:T(8,128)(2,1)S(1)}, bf16[768,256]{1,0:T(8,128)(2,1)S(1)}) fusion(f32[768,256]{1,0:T(8,128)} %fusion.2, f32[768,256]{1,0:T(8,128)} %fusion.5, bf16[768,4096]{0,1:T(8,128)(2,1)} %bitcast.10, bf16[1,256,4096]{2,1,0:T(8,128)(2,1)} %param.21), kind=kOutput, calls=%fused_computation.54 | convolution fusion | flops 1613168640 | bytes 10747904 | tf_op jit(solution)/shard_map/dot_general | solution.py:109
  250.0 6.6 %convolution_add_fusion = f32[768,4096]{1,0:T(8,128)} fusion(f32[768,4096]{1,0:T(8,128)S(1)} %fusion, bf16[768,256]{1,0:T(8,128)(2,1)S(1)} %get-tuple-element.47, bf16[1,4096,256]{2,1,0:T(8,128)(2,1)S(1)} %copy-done.5), kind=kOutput, calls=%fused_computation.2 | convolution fusion | flops 1613758464 | bytes 27656192 | tf_op jit(solution)/shard_map/dot_general | solution.py:125
  256.7 127.8 %reduce-scatter.3.cloned.1.call-done = f32[768,512]{1,0:T(8,128)} async-done(((f32[768,4096]{1,0:T(8,128)}), f32[768,512]{1,0:T(8,128)}) %reduce-scatter.3.cloned.1.call-update) | async-done | bytes 1572880 | tf_op jit(solution)/shard_map/reduce_scatter | solution.py:128
  386.9 3.6 all-to-all-start.3
  390.7 8.9 %all-to-all-done.3 = bf16[4,192,512]{2,1,0:T(8,128)(2,1)S(1)} async-done(((bf16[4,192,512]{2,1,0:T(8,128)(2,1)}), bf16[4,192,512]{2,1,0:T(8,128)(2,1)S(1)}, u32[]{:S(2)}, u32[]{:S(2)}) %all-to-all-start.3) | async-done | bytes 786464 | tf_op jit(solution)/shard_map/all_to_all | solution.py:131
  400.1 14.8 %all-reduce.3 = (f32[256]{0:T(256)S(1)}, f32[256]{0:T(256)S(1)}, f32[256]{0:T(256)S(1)}) all-reduce(f32[256]{0:T(256)S(1)} %get-tuple-element.88, f32[256]{0:T(256)S(1)} %get-tuple-element.39, f32[256]{0:T(256)S(1)} %get-tuple-element.38), channel_id=1, replica_groups=mesh['sp'=4,'tp'=8] {'tp'}, use_global_device_ids=true, to_apply=%region_10.11 | all-reduce | flops 768 | bytes 6144 | tf_op jit(solution)/shard_map/psum | solution.py:143
  416.2 25.9 %all-gather.5.cloned.1.call-done = bf16[256,4096]{1,0:T(8,128)(2,1)} async-done(((bf16[256,512]{1,0:T(8,128)(2,1)}), bf16[256,4096]{1,0:T(8,128)(2,1)}) %all-gather.5.cloned.1.call-update) | async-done | bytes 2097168 | tf_op jit(solution)/shard_map/all_gather | solution.py:146
  442.0 4.4 fusion.132
  447.4 6.8 %convolution_bitcast_fusion.2 = f32[1,4096,256]{2,1,0:T(8,128)} fusion(bf16[768,4096]{1,0:T(8,128)(2,1)} %all-gather.3.cloned.1.call-done, bf16[768,256]{1,0:T(8,128)(2,1)S(1)} %copy-done.10), kind=kOutput, calls=%fused_computation.5 | convolution fusion | flops 1610612736 | bytes 10878976 | tf_op jit(solution)/shard_map/dot_general | solution.py:114
  454.2 6.9 %convolution_bitcast_fusion = f32[1,256,4096]{2,1,0:T(8,128)} fusion(bf16[768,4096]{0,1:T(8,128)(2,1)} %bitcast.10, f32[768,256]{1,0:T(8,128)S(1)} %copy-done.19, f32[768,256]{1,0:T(8,128)S(1)} %copy-done.18), kind=kOutput, calls=%fused_computation.3 | convolution fusion | flops 1611792384 | bytes 12058624 | tf_op jit(solution)/shard_map/dot_general | solution.py:120
  461.9 15.3 %all-reduce.2 = (f32[256]{0:T(256)S(1)}, f32[256]{0:T(256)S(1)}) all-reduce(f32[256]{0:T(256)S(1)} %get-tuple-element.37, f32[256]{0:T(256)S(1)} %get-tuple-element.36), channel_id=1, replica_groups=mesh['sp'=4,'tp'=8] {'tp'}, use_global_device_ids=true, to_apply=%region_19.20 | all-reduce | flops 512 | bytes 4096 | tf_op jit(solution)/shard_map/psum | solution.py:167
  478.9 6.8 %convolution_bitcast_fusion.1 = f32[1,4096,256]{2,1,0:T(8,128)} fusion(bf16[768,4096]{1,0:T(8,128)(2,1)} %all-gather.3.cloned.1.call-done, bf16[768,256]{1,0:T(8,128)(2,1)S(1)} %get-tuple-element.47), kind=kOutput, calls=%fused_computation.4 | convolution fusion | flops 1610612736 | bytes 10878976 | tf_op jit(solution)/shard_map/dot_general | solution.py:117
  488.6 10.0 %reduce-scatter.5.cloned.1.call-done = f32[1024,256]{1,0:T(8,128)} async-done(((f32[4096,256]{1,0:T(8,128)}), f32[1024,256]{1,0:T(8,128)}) %reduce-scatter.5.cloned.1.call-update) | async-done | bytes 1048592 | tf_op jit(solution)/shard_map/reduce_scatter | solution.py:154
  (94 shorter events, 23.8 us)
Async XLA Ops:
  7.2 133.4 %copy-start = (bf16[1,4096,256]{2,1,0:T(8,128)(2,1)S(1)}, bf16[1,4096,256]{2,1,0:T(8,128)(2,1)}, u32[]{:S(2)}) copy-start(bf16[1,4096,256]{2,1,0:T(8,128)(2,1)} %param.19) | copy-start | bytes 6291460
  7.2 133.3 %all-gather.3.cloned.1.call-start = ((), (), s32[]{:S(2)}) async-start(), calls=%async_computation.6 | async-start | bytes 7077888 | tf_op jit(solution)/shard_map/all_gather | solution.py:92
  31.9 14.9 %copy-start.7 = (bf16[256,512]{1,0:T(8,128)(2,1)S(1)}, bf16[256,512]{1,0:T(8,128)(2,1)}, u32[]{:S(2)}) copy-start(bf16[256,512]{1,0:T(8,128)(2,1)} %param.14) | copy-start | bytes 786436
  46.8 2.8 copy-start.14
  66.2 176.2 %all-to-all-start.2 = ((bf16[8,768,512]{1,2,0:T(8,128)(2,1)}), bf16[8,768,512]{1,2,0:T(8,128)(2,1)}, u32[]{:S(2)}, u32[]{:S(2)}) async-start(bf16[8,768,512]{1,2,0:T(8,128)(2,1)} %stack.3), calls=%async_computation.2 | async-start | bytes 12582912 | tf_op jit(solution)/shard_map/all_to_all | solution.py:94
  72.7 311.8 %reduce-scatter.3.cloned.1.call-start = ((), (), s32[]{:S(2)}) async-start(), calls=%async_computation.7 | async-start | bytes 14155776 | tf_op jit(solution)/shard_map/reduce_scatter | solution.py:128
  140.5 5.6 %copy-start.4 = (bf16[1,4096,256]{2,1,0:T(8,128)(2,1)S(1)}, bf16[1,4096,256]{2,1,0:T(8,128)(2,1)}, u32[]{:S(2)}) copy-start(bf16[1,4096,256]{2,1,0:T(8,128)(2,1)} %param.20) | copy-start | bytes 6291460
  140.5 5.6 %copy-start.16 = (bf16[768,4096]{1,0:T(8,128)(2,1)S(1)}, bf16[768,4096]{1,0:T(8,128)(2,1)}, u32[]{:S(2)}) copy-start(bf16[768,4096]{1,0:T(8,128)(2,1)} %all-gather.3.cloned.1.call-done) | copy-start | bytes 18874372
  248.2 1.9 copy-start.9
  256.6 133.9 %copy-start.6 = (bf16[256,256]{1,0:T(8,128)(2,1)S(1)}, bf16[256,256]{1,0:T(8,128)(2,1)}, u32[]{:S(2)}) copy-start(bf16[256,256]{1,0:T(8,128)(2,1)} %param.24) | copy-start | bytes 393220
  256.6 143.0 %copy-start.3 = (bf16[256,512]{1,0:T(8,128)(2,1)S(1)}, bf16[256,512]{1,0:T(8,128)(2,1)}, u32[]{:S(2)}) copy-start(bf16[256,512]{1,0:T(8,128)(2,1)} %param.15) | copy-start | bytes 786436
  256.6 143.0 %copy-start.13 = (f32[512]{0:T(512)S(1)}, f32[512]{0:T(512)}, u32[]{:S(2)}) copy-start(f32[512]{0:T(512)} %param.16) | copy-start | bytes 6148
  256.7 185.4 %copy-start.15 = (f32[256]{0:T(256)S(1)}, f32[256]{0:T(256)}, u32[]{:S(2)}) copy-start(f32[256]{0:T(256)} %param.25) | copy-start | bytes 3076
  386.9 12.7 %all-to-all-start.3 = ((bf16[4,192,512]{2,1,0:T(8,128)(2,1)}), bf16[4,192,512]{2,1,0:T(8,128)(2,1)S(1)}, u32[]{:S(2)}, u32[]{:S(2)}) async-start(bf16[4,192,512]{2,1,0:T(8,128)(2,1)} %bitcast.18), calls=%async_computation.4 | async-start | bytes 1572864 | tf_op jit(solution)/shard_map/all_to_all | solution.py:131
  390.5 51.5 %all-gather.5.cloned.1.call-start = ((), (), s32[]{:S(2)}) async-start(), calls=%async_computation.8 | async-start | bytes 2359296 | tf_op jit(solution)/shard_map/all_gather | solution.py:146
  415.9 82.7 %reduce-scatter.5.cloned.1.call-start = ((), (), s32[]{:S(2)}) async-start(), calls=%async_computation.9 | async-start | bytes 5242880 | tf_op jit(solution)/shard_map/reduce_scatter | solution.py:154
  447.4 6.8 %copy-start.18 = (f32[768,256]{1,0:T(8,128)S(1)}, f32[768,256]{1,0:T(8,128)}, u32[]{:S(2)}) copy-start(f32[768,256]{1,0:T(8,128)} %fusion.2) | copy-start | bytes 2359300
  447.4 6.8 %copy-start.19 = (f32[768,256]{1,0:T(8,128)S(1)}, f32[768,256]{1,0:T(8,128)}, u32[]{:S(2)}) copy-start(f32[768,256]{1,0:T(8,128)} %fusion.5) | copy-start | bytes 2359300
  454.2 6.9 %copy-start.2 = (bf16[256,4096]{1,0:T(8,128)(2,1)S(1)}, bf16[256,4096]{1,0:T(8,128)(2,1)}, u32[]{:S(2)}) copy-start(bf16[256,4096]{1,0:T(8,128)(2,1)} %all-gather.5.cloned.1.call-done) | copy-start | bytes 6291460
  454.2 6.9 %copy-start.17 = (bf16[256,4096]{1,0:T(8,128)(2,1)S(1)}, bf16[256,4096]{1,0:T(8,128)(2,1)}, u32[]{:S(2)}) copy-start(bf16[256,4096]{1,0:T(8,128)(2,1)} %param.27) | copy-start | bytes 6291460
  477.5 8.3 %copy-start.8 = (bf16[256,256]{1,0:T(8,128)(2,1)S(1)}, bf16[256,256]{1,0:T(8,128)(2,1)}, u32[]{:S(2)}) copy-start(bf16[256,256]{1,0:T(8,128)(2,1)} %param.23) | copy-start | bytes 393220
  477.5 8.2 %copy-start.11 = (bf16[256,256]{1,0:T(8,128)(2,1)S(1)}, bf16[256,256]{1,0:T(8,128)(2,1)}, u32[]{:S(2)}) copy-start(bf16[256,256]{1,0:T(8,128)(2,1)} %param.22) | copy-start | bytes 393220
  477.5 8.2 %collective-permute-start = (f32[30,256]{1,0:T(8,128)S(1)}, f32[30,256]{1,0:T(8,128)S(1)}, u32[]{:S(2)}, u32[]{:S(2)}) collective-permute-start(f32[30,256]{1,0:T(8,128)S(1)} %slice.279), channel_id=1, source_target_pairs={{8,0},{16,8},{24,16},{9,1},{17,9},{25,17},{10,2},{18,10},{26,18},{... | collective-permute-start | bytes 92168 | tf_op jit(solution)/shard_map/ppermute | solution.py:12
  478.9 22.2 %copy-start.1 = (bf16[1,4096,256]{2,1,0:T(8,128)(2,1)S(1)}, bf16[1,4096,256]{2,1,0:T(8,128)(2,1)}, u32[]{:S(2)}) copy-start(bf16[1,4096,256]{2,1,0:T(8,128)(2,1)} %param.19) | copy-start | bytes 6291460
  (3 other events, 3.6 us)
Sparse Core Ops, SparseCore 0:
  46.9 93.5 all-gather.2
  256.8 127.6 reduce-scatter.2
  416.0 25.9 all-gather.4
  446.6 51.9 reduce-scatter.4
